TPU v7x, 256 devices: a whole 4x4x8 slice. The times are simulated.
256 devices in a mesh: sp: 16 (over y, x), dp: 16 (over z, core).
Axes of the slice: x: 4, y: 4, z: 8, core: 2. Of those that a mesh axis runs over, the one named last changes fastest.
Arguments:
- tokens: bfloat16 [16, 2048, 2048], P('dp', 'sp'), may hold values from -6 to 6
- query_weight: bfloat16 [2048, 1024], P('dp'), may hold values from -0.125 to 0.125
- key_weight: bfloat16 [2048, 1024], P('dp'), may hold values from -0.125 to 0.125
- value_weight: bfloat16 [2048, 2048], P('dp'), may hold values from -0.125 to 0.125
- output_weight: bfloat16 [2048, 2048], P('dp'), may hold values from -0.125 to 0.125
- log_decay: float32 [2, 16], P(None, 'sp'), may hold values from -0.04 to 0, as said below
Outputs:
- mixed: bfloat16 [16, 2048, 2048], P('dp', 'sp')
Inputs may be any that keep to these rules, and one draw needn't show every extreme that they name: `log_decay`: every entry is negative: the logarithm of a head's decay per position.
All inputs are finite; a program needn't handle non-finite values.
Results may differ from a plain program's by a relative error of at most 0.012.
Values may be sent and summed in bfloat16 or wider, within the bound.
No kernel may reach another device: no remote copies, remote signals or barrier semaphores. Data moves between devices by JAX's collectives and lax.ppermute only.
A program may use at most 128 MiB of HBM per device.

v0:
```python
import jax
import jax.numpy as jnp
from jax import lax
from jax.sharding import PartitionSpec as P

HEADS = 16
DK = 64
DV = 128
BLOCK = 512


def in_order(pieces, dim):
    lengths = list(pieces.shape[1:])
    lengths[dim] *= pieces.shape[0]
    return jnp.moveaxis(pieces, 0, dim).reshape(lengths)


def copy_for_each(shard, axis):
    count = lax.axis_size(axis)
    return lax.all_to_all(
        jnp.broadcast_to(shard[None], (count, *shard.shape)), axis, 0, 0, tiled=True
    )


def gathered_copies(shard, axis, dim):
    return in_order(copy_for_each(shard, axis), dim)


def rotate(values_part, positions):
    half_dim = values_part.shape[-1] // 2
    frequency = 10000.0 ** (-jnp.arange(half_dim, dtype=jnp.float32) / half_dim)
    angles = positions[:, None] * frequency[None, :]
    cosine = jnp.cos(angles)[:, None, :]
    sine_part = jnp.sin(angles)[:, None, :]
    first = values_part[..., :half_dim]
    second = values_part[..., half_dim:]
    return jnp.concatenate(
        [first * cosine - second * sine_part, first * sine_part + second * cosine], axis=-1
    )


def retain(query, key_rows, value_rows, log_rate):
    length, heads, key_dim = query.shape
    value_dim = value_rows.shape[-1]
    count = length // BLOCK
    offsets = jnp.arange(BLOCK, dtype=jnp.float32)
    distance = offsets[:, None] - offsets[None, :]
    decay_inner = jnp.where(
        distance[None] >= 0.0,
        jnp.exp(log_rate[:, None, None] * jnp.maximum(distance, 0.0)[None]),
        0.0,
    )
    decay_query = jnp.exp((offsets[:, None] + 1.0) * log_rate[None, :])[:, :, None]
    decay_key = jnp.exp((BLOCK - 1.0 - offsets)[:, None] * log_rate[None, :])[:, :, None]
    decay_block = jnp.exp(BLOCK * log_rate)[:, None, None]

    def blocks(array):
        return array.reshape(count, BLOCK, heads, array.shape[-1])

    def advance(state, inputs):
        query_block, key_block, value_block = inputs
        inner = (
            jnp.einsum("ihd,jhd->hij", query_block, key_block, preferred_element_type=jnp.float32)
            * decay_inner
        )
        result = jnp.einsum(
            "hij,jhv->ihv",
            inner.astype(jnp.bfloat16),
            value_block,
            preferred_element_type=jnp.float32,
        )
        query_wide = query_block.astype(jnp.float32) * decay_query
        result = result + jnp.einsum("ihd,hdv->ihv", query_wide, state)
        key_wide = key_block.astype(jnp.float32) * decay_key
        state = state * decay_block + jnp.einsum(
            "jhd,jhv->hdv", key_wide, value_block.astype(jnp.float32)
        )
        return (state, result)

    initial = jnp.zeros((heads, key_dim, value_dim), jnp.float32)
    final_state, outputs = lax.scan(
        advance, initial, (blocks(query), blocks(key_rows), blocks(value_rows))
    )
    return outputs.reshape(length, heads, value_dim)


def mechanism(stacked, log_decay):
    length = stacked.shape[0]
    widened = stacked[..., : 2 * DK].astype(jnp.float32)
    positions = jnp.arange(length, dtype=jnp.float32)
    query = rotate(widened[..., :DK], positions).astype(jnp.bfloat16)
    key_rows = rotate(widened[..., DK : 2 * DK], positions).astype(jnp.bfloat16)
    value_rows = stacked[..., 2 * DK :]
    forward = retain(query, key_rows, value_rows, log_decay[0])
    backward = retain(
        jnp.flip(query, 0), jnp.flip(key_rows, 0), jnp.flip(value_rows, 0), log_decay[1]
    )
    combined = forward + jnp.flip(backward, 0)
    average = jnp.mean(combined, axis=-1, keepdims=True)
    centred = combined - average
    variance = jnp.mean(centred * centred, axis=-1, keepdims=True)
    return (centred * lax.rsqrt(variance + 1e-06)).astype(jnp.bfloat16)


def shards(tokens, query_weight, key_weight, value_weight, output_weight, log_decay):
    rows = tokens[0]
    row_count = rows.shape[0]
    local_heads = log_decay.shape[1]
    first_head = lax.axis_index("sp") * local_heads
    own_slices = jnp.concatenate(
        [
            lax.dynamic_slice_in_dim(query_weight, first_head * DK, local_heads * DK, 1),
            lax.dynamic_slice_in_dim(key_weight, first_head * DK, local_heads * DK, 1),
            lax.dynamic_slice_in_dim(value_weight, first_head * DV, local_heads * DV, 1),
        ],
        axis=1,
    )
    own_whole = gathered_copies(own_slices, "dp", 0)
    piece = lax.all_gather(rows, "sp", axis=0, tiled=True)
    count = piece.shape[0]
    product = jnp.dot(piece, own_whole, preferred_element_type=jnp.float32).astype(jnp.bfloat16)
    query_part = product[:, : local_heads * DK].reshape(count, local_heads, DK)
    key_part = product[:, local_heads * DK : 2 * local_heads * DK].reshape(count, local_heads, DK)
    value_part = product[:, 2 * local_heads * DK :].reshape(count, local_heads, DV)
    gathered = jnp.concatenate([query_part, key_part, value_part], axis=2)
    normed = mechanism(gathered, log_decay)
    by_token = lax.all_to_all(normed, "sp", split_axis=0, concat_axis=1, tiled=True).reshape(
        row_count, HEADS * DV
    )
    mixed = jnp.dot(
        by_token,
        lax.all_gather(output_weight, "dp", axis=0, tiled=True),
        preferred_element_type=jnp.float32,
    )
    return mixed.astype(jnp.bfloat16)[None]


def solution(mesh):
    placed = (
        P("dp", "sp", None),
        P("dp", None),
        P("dp", None),
        P("dp", None),
        P("dp", None),
        P(None, "sp"),
    )
    return jax.shard_map(
        shards, mesh=mesh, in_specs=placed, out_specs=P("dp", "sp", None), check_vma=False
    )
```

profile of v0, /device:TPU:32, one launch (start us, length us, event | category | flops | bytes accessed | tf_op | source)
XLA Modules:
  0.0 171.1 jit_solution(11749039148471384118)
XLA Ops:
  10.1 8.6 %all-to-all-start = ((bf16[16,128,256]{2,1,0:T(8,128)(2,1)}), bf16[16,128,256]{2,1,0:T(8,128)(2,1)S(1)}, u32[]{:S(2)}, u32[]{:S(2)}) async-start(bf16[16,128,256]{2,1,0:T(8,128)(2,1)} %broadcast_in_dim.18), calls=%async_computation | async-start | bytes 2097152 | tf_op jit(solution)/shard_map/all_to_all | solution.py:20
  18.7 1.4 fusion.116
  21.5 21.8 %all-to-all-done = bf16[16,128,256]{2,1,0:T(8,128)(2,1)S(1)} async-done(((bf16[16,128,256]{2,1,0:T(8,128)(2,1)}), bf16[16,128,256]{2,1,0:T(8,128)(2,1)S(1)}, u32[]{:S(2)}, u32[]{:S(2)}) %all-to-all-start) | async-done | bytes 1048608 | tf_op jit(solution)/shard_map/all_to_all | solution.py:20
  43.3 45.0 %all-gather.6.cloned.1.call-done = bf16[1,2048,2048]{2,1,0:T(8,128)(2,1)} async-done(((bf16[1,128,2048]{2,1,0:T(8,128)(2,1)}), bf16[1,2048,2048]{2,1,0:T(8,128)(2,1)}) %all-gather.6.cloned.1.call-update) | async-done | bytes 8388624 | tf_op jit(solution)/shard_map/all_gather | solution.py:119
  88.3 5.8 %fusion.109 = bf16[2048,256]{0,1:T(8,128)(2,1)S(1)} fusion(bf16[2048,256]{1,0:T(8,128)(2,1)S(1)} %bitcast.255, bf16[1,2048,2048]{2,1,0:T(8,128)(2,1)} %all-gather.6.cloned.1.call-done), kind=kOutput, calls=%fused_computation.103 | convolution fusion | flops 2148007936 | bytes 10485760 | tf_op jit(solution)/shard_map/dot_general | solution.py:121
  95.1 1.6 reverse.3
  96.9 1.2 subtract_convert_fusion
  98.3 1.4 rev.14
  99.7 1.4 rev.13
  102.2 17.2 %while.31 = (s32[]{:T(128)}, f32[1,64,128]{2,1,0:T(8,128)S(1)}, f32[4,512,1,128]{3,1,0,2:T(8,128)S(1)}, f32[1,1,1]{2,1,0:T(1,128)}, bf16[4,512,1,64]{1,3,2,0:T(8...) while((s32[]{:T(128)}, f32[1,64,128]{2,1,0:T(8,128)S(1)}, ...), condition=%wide.region_3.4_spmd.clone.clone.clone, body=%wide.region_2.3_spmd.clone.clone.clone.sunk | while | flops 119506944 | bytes 2469500 | solution.py:81
  102.2 2.2 %fusion.158 = f32[128,512]{1,0:T(8,128)S(1)} fusion(f32[]{:T(128)} %get-tuple-element.508, bf16[4,512,1,128]{3,1,2,0:T(8,128)(2,1)S(1)} %get-tuple-element.506, s32[]{:T(128)} %get-tuple-element.491, bf16[4,512,1,64]{1,3,2,0:T(8,128)(2,1)S(1)} %get-tuple-element.507, bf16[4,512,1,64]{1,3,2,0:T(8,128)(2,1)} %get-tuple-element.505), kind=kOutput, calls=%fused_computation.55.clone.1 | convolution fusion | flops 102498304 | bytes 526336 | tf_op jit(solution)/shard_map/while/body/eval_jaxpr/hij,jhv->ihv/dot_general | solution.py:66
  106.5 2.2 %fusion.158 = f32[128,512]{1,0:T(8,128)S(1)} fusion(f32[]{:T(128)} %get-tuple-element.508, bf16[4,512,1,128]{3,1,2,0:T(8,128)(2,1)S(1)} %get-tuple-element.506, s32[]{:T(128)} %get-tuple-element.491, bf16[4,512,1,64]{1,3,2,0:T(8,128)(2,1)S(1)} %get-tuple-element.507, bf16[4,512,1,64]{1,3,2,0:T(8,128)(2,1)} %get-tuple-element.505), kind=kOutput, calls=%fused_computation.55.clone.1 | convolution fusion | flops 102498304 | bytes 526336 | tf_op jit(solution)/shard_map/while/body/eval_jaxpr/hij,jhv->ihv/dot_general | solution.py:66
  110.9 2.2 %fusion.158 = f32[128,512]{1,0:T(8,128)S(1)} fusion(f32[]{:T(128)} %get-tuple-element.508, bf16[4,512,1,128]{3,1,2,0:T(8,128)(2,1)S(1)} %get-tuple-element.506, s32[]{:T(128)} %get-tuple-element.491, bf16[4,512,1,64]{1,3,2,0:T(8,128)(2,1)S(1)} %get-tuple-element.507, bf16[4,512,1,64]{1,3,2,0:T(8,128)(2,1)} %get-tuple-element.505), kind=kOutput, calls=%fused_computation.55.clone.1 | convolution fusion | flops 102498304 | bytes 526336 | tf_op jit(solution)/shard_map/while/body/eval_jaxpr/hij,jhv->ihv/dot_general | solution.py:66
  115.2 2.2 %fusion.158 = f32[128,512]{1,0:T(8,128)S(1)} fusion(f32[]{:T(128)} %get-tuple-element.508, bf16[4,512,1,128]{3,1,2,0:T(8,128)(2,1)S(1)} %get-tuple-element.506, s32[]{:T(128)} %get-tuple-element.491, bf16[4,512,1,64]{1,3,2,0:T(8,128)(2,1)S(1)} %get-tuple-element.507, bf16[4,512,1,64]{1,3,2,0:T(8,128)(2,1)} %get-tuple-element.505), kind=kOutput, calls=%fused_computation.55.clone.1 | convolution fusion | flops 102498304 | bytes 526336 | tf_op jit(solution)/shard_map/while/body/eval_jaxpr/hij,jhv->ihv/dot_general | solution.py:66
  120.7 17.5 %while.30 = (s32[]{:T(128)}, f32[1,64,128]{2,1,0:T(8,128)S(1)}, f32[4,512,1,128]{3,1,0,2:T(8,128)S(1)}, f32[1,1,1]{2,1,0:T(1,128)}, bf16[4,512,1,64]{1,3,2,0:T(8...) while((s32[]{:T(128)}, f32[1,64,128]{2,1,0:T(8,128)S(1)}, ...), condition=%wide.region_1.2_spmd.clone.clone.clone, body=%wide.region_0.1_spmd.clone.clone.clone.sunk | while | flops 119506944 | bytes 2469500 | solution.py:81
  120.7 2.2 %fusion.148 = f32[128,512]{1,0:T(8,128)S(1)} fusion(f32[]{:T(128)} %get-tuple-element.538, bf16[4,512,1,128]{3,1,2,0:T(8,128)(2,1)} %get-tuple-element.536, s32[]{:T(128)} %get-tuple-element.521, bf16[4,512,1,64]{1,3,2,0:T(8,128)(2,1)S(1)} %get-tuple-element.537, bf16[4,512,1,64]{1,3,2,0:T(8,128)(2,1)} %get-tuple-element.535), kind=kOutput, calls=%fused_computation.8.clone.1 | convolution fusion | flops 102498304 | bytes 526336 | tf_op jit(solution)/shard_map/while/body/eval_jaxpr/hij,jhv->ihv/dot_general | solution.py:66
  124.0 1.1 fusion.147
  125.1 2.2 %fusion.148 = f32[128,512]{1,0:T(8,128)S(1)} fusion(f32[]{:T(128)} %get-tuple-element.538, bf16[4,512,1,128]{3,1,2,0:T(8,128)(2,1)} %get-tuple-element.536, s32[]{:T(128)} %get-tuple-element.521, bf16[4,512,1,64]{1,3,2,0:T(8,128)(2,1)S(1)} %get-tuple-element.537, bf16[4,512,1,64]{1,3,2,0:T(8,128)(2,1)} %get-tuple-element.535), kind=kOutput, calls=%fused_computation.8.clone.1 | convolution fusion | flops 102498304 | bytes 526336 | tf_op jit(solution)/shard_map/while/body/eval_jaxpr/hij,jhv->ihv/dot_general | solution.py:66
  128.3 1.1 fusion.147
  129.4 2.2 %fusion.148 = f32[128,512]{1,0:T(8,128)S(1)} fusion(f32[]{:T(128)} %get-tuple-element.538, bf16[4,512,1,128]{3,1,2,0:T(8,128)(2,1)} %get-tuple-element.536, s32[]{:T(128)} %get-tuple-element.521, bf16[4,512,1,64]{1,3,2,0:T(8,128)(2,1)S(1)} %get-tuple-element.537, bf16[4,512,1,64]{1,3,2,0:T(8,128)(2,1)} %get-tuple-element.535), kind=kOutput, calls=%fused_computation.8.clone.1 | convolution fusion | flops 102498304 | bytes 526336 | tf_op jit(solution)/shard_map/while/body/eval_jaxpr/hij,jhv->ihv/dot_general | solution.py:66
  132.7 1.1 fusion.147
  133.8 2.2 %fusion.148 = f32[128,512]{1,0:T(8,128)S(1)} fusion(f32[]{:T(128)} %get-tuple-element.538, bf16[4,512,1,128]{3,1,2,0:T(8,128)(2,1)} %get-tuple-element.536, s32[]{:T(128)} %get-tuple-element.521, bf16[4,512,1,64]{1,3,2,0:T(8,128)(2,1)S(1)} %get-tuple-element.537, bf16[4,512,1,64]{1,3,2,0:T(8,128)(2,1)} %get-tuple-element.535), kind=kOutput, calls=%fused_computation.8.clone.1 | convolution fusion | flops 102498304 | bytes 526336 | tf_op jit(solution)/shard_map/while/body/eval_jaxpr/hij,jhv->ihv/dot_general | solution.py:66
  141.5 16.4 %all_to_all.20 = bf16[16,2,8192]{2,1,0:T(2,128)(2,1)S(1)} all-to-all(bf16[16,2,8192]{2,1,0:T(2,128)(2,1)S(1)} %reshape.742), channel_id=1, replica_groups=mesh['sp'=16,'dp'=16] {'sp'}, dimensions={0} | all-to-all | bytes 1048576 | tf_op jit(solution)/shard_map/all_to_all | solution.py:127
  158.8 5.5 %fusion.112 = bf16[1,128,2048]{2,1,0:T(8,128)(2,1)} fusion(bf16[128,2048]{0,1:T(8,128)(2,1)S(1)} %bitcast.246, bf16[2048,2048]{1,0:T(8,128)(2,1)} %all-gather.4.cloned.1.call-done), kind=kOutput, calls=%fused_computation.105 | convolution fusion | flops 1074003968 | bytes 9437184 | tf_op jit(solution)/shard_map/dot_general | solution.py:130
  (80 shorter events, 24.7 us)
Async XLA Ops:
  6.5 1.5 copy-start
  6.5 81.7 %all-gather.6.cloned.1.call-start = ((), (), s32[]{:S(2)}) async-start(), calls=%async_computation.3 | async-start | bytes 8912896 | tf_op jit(solution)/shard_map/all_gather | solution.py:119
  7.3 151.5 %all-gather.4.cloned.1.call-start = ((), (), s32[]{:S(2)}) async-start(), calls=%async_computation.2 | async-start | bytes 8912896 | tf_op jit(solution)/shard_map/all_gather | solution.py:132
  10.1 33.2 %all-to-all-start = ((bf16[16,128,256]{2,1,0:T(8,128)(2,1)}), bf16[16,128,256]{2,1,0:T(8,128)(2,1)S(1)}, u32[]{:S(2)}, u32[]{:S(2)}) async-start(bf16[16,128,256]{2,1,0:T(8,128)(2,1)} %broadcast_in_dim.18), calls=%async_computation | async-start | bytes 2097152 | tf_op jit(solution)/shard_map/all_to_all | solution.py:20
Sparse Core Ops, SparseCore 0:
  9.8 78.4 all-gather.5
  90.1 53.8 all-gather.3
where the time goes:
time: 172 us; the launch traced here: 171 us
  waiting for transfers between devices  68.2 us (40%)
  matrix products  39 us (23%)
  blocking collectives  16.4 us (10%)
  between operations  15 us (9%)
  local copies, waits for them, and re-layouts  13.2 us (8%)
  other arithmetic  10.2 us (6%)
  starting transfers between devices  8.63 us (5%)
    all_gather x1, waiting for transfers between devices, shards(): piece = lax.all_gather(rows, 'sp', axis=0, tiled=True)  45 us
    all_to_all x1, waiting for transfers between devices, copy_for_each(): lax.all_to_all(jnp.broadcast_to(shard[None], (count, *shard.shape)), axis...  21.8 us
    dot_general x8, matrix products, advance(): jnp.einsum('hij,jhv->ihv', inner.astype(jnp.bfloat16), value_block, prefe...  17.5 us
    all_to_all x1, blocking collectives, shards(): lax.all_to_all(normed, 'sp', split_axis=0, concat_axis=1, tiled=True)  16.4 us
    all_to_all x1, starting transfers between devices, copy_for_each(): lax.all_to_all(jnp.broadcast_to(shard[None], (count, *shard.shape)), axis...  8.59 us
    dot_general x8, matrix products, advance(): jnp.einsum('jhd,jhv->hdv', key_wide, value_block.astype(jnp.float32))  8.43 us
    dot_general x1, matrix products, shards(): jnp.dot(piece, own_whole, preferred_element_type=jnp.float32)  5.77 us
    dot_general x1, matrix products, shards(): jnp.dot(by_token, lax.all_gather(output_weight, 'dp', axis=0, tiled=True)...  5.47 us
  transfers between devices with their start and end apart: 3, of which 2 were waited for; matrix products, arithmetic and copies ran while one was open for 33% of the time, Pallas kernels for 0%

commit v1 on v0

--- a/solution.py
+++ b/solution.py
@@ -124,9 +124,10 @@
     value_part = product[:, 2 * local_heads * DK :].reshape(count, local_heads, DV)
     gathered = jnp.concatenate([query_part, key_part, value_part], axis=2)
     normed = mechanism(gathered, log_decay)
-    by_token = lax.all_to_all(normed, "sp", split_axis=0, concat_axis=1, tiled=True).reshape(
-        row_count, HEADS * DV
-    )
+    by_token = jnp.concatenate(
+        lax.all_to_all(jnp.stack(jnp.split(normed, lax.axis_size("sp"), axis=0)), "sp", 0, 0),
+        axis=1,
+    ).reshape(row_count, HEADS * DV)
     mixed = jnp.dot(
         by_token,
         lax.all_gather(output_weight, "dp", axis=0, tiled=True),

time: 172 us -> 170 us (0.988)
  transfers between devices with their start and end apart: 3 -> 3, of which waited for: 2 -> 2; matrix products, arithmetic and copies ran while one was open for 33% -> 32% of each run, Pallas kernels for 0% -> 0%
where the time goes in v1:
time: 170 us; the launch traced here: 169 us
  waiting for transfers between devices  68.4 us (40%)
  matrix products  38.8 us (23%)
  blocking collectives  16.4 us (10%)
  between operations  15.1 us (9%)
  local copies, waits for them, and re-layouts  12 us (7%)
  other arithmetic  8.94 us (5%)
  starting transfers between devices  8.63 us (5%)
    all_gather x1, waiting for transfers between devices, shards(): piece = lax.all_gather(rows, 'sp', axis=0, tiled=True)  45 us
    all_to_all x1, waiting for transfers between devices, copy_for_each(): lax.all_to_all(jnp.broadcast_to(shard[None], (count, *shard.shape)), axis...  21.9 us
    dot_general x8, matrix products, advance(): jnp.einsum('hij,jhv->ihv', inner.astype(jnp.bfloat16), value_block, prefe...  17.3 us
    all_to_all x1, blocking collectives, shards(): lax.all_to_all(jnp.stack(jnp.split(normed, lax.axis_size('sp'), axis=0)),...  16.4 us
    all_to_all x1, starting transfers between devices, copy_for_each(): lax.all_to_all(jnp.broadcast_to(shard[None], (count, *shard.shape)), axis...  8.59 us
    dot_general x8, matrix products, advance(): jnp.einsum('jhd,jhv->hdv', key_wide, value_block.astype(jnp.float32))  8.46 us
    dot_general x1, matrix products, shards(): jnp.dot(piece, own_whole, preferred_element_type=jnp.float32)  5.77 us
    dot_general x1, matrix products, shards(): jnp.dot(by_token, lax.all_gather(output_weight, 'dp', axis=0, tiled=True)...  5.46 us
  transfers between devices with their start and end apart: 3, of which 2 were waited for; matrix products, arithmetic and copies ran while one was open for 32% of the time, Pallas kernels for 0%

profile of v1, /device:TPU:32, one launch (start us, length us, event | category | flops | bytes accessed | tf_op | source)
XLA Modules:
  0.0 168.7 jit_solution(14280036012243845060)
XLA Ops:
  10.1 8.6 %all-to-all-start = ((bf16[16,128,256]{2,1,0:T(8,128)(2,1)}), bf16[16,128,256]{2,1,0:T(8,128)(2,1)S(1)}, u32[]{:S(2)}, u32[]{:S(2)}) async-start(bf16[16,128,256]{2,1,0:T(8,128)(2,1)} %broadcast_in_dim.18), calls=%async_computation | async-start | bytes 2097152 | tf_op jit(solution)/shard_map/all_to_all | solution.py:20
  18.7 1.3 fusion.116
  21.4 21.9 %all-to-all-done = bf16[16,128,256]{2,1,0:T(8,128)(2,1)S(1)} async-done(((bf16[16,128,256]{2,1,0:T(8,128)(2,1)}), bf16[16,128,256]{2,1,0:T(8,128)(2,1)S(1)}, u32[]{:S(2)}, u32[]{:S(2)}) %all-to-all-start) | async-done | bytes 1048608 | tf_op jit(solution)/shard_map/all_to_all | solution.py:20
  43.3 45.0 %all-gather.6.cloned.1.call-done = bf16[1,2048,2048]{2,1,0:T(8,128)(2,1)} async-done(((bf16[1,128,2048]{2,1,0:T(8,128)(2,1)}), bf16[1,2048,2048]{2,1,0:T(8,128)(2,1)}) %all-gather.6.cloned.1.call-update) | async-done | bytes 8388624 | tf_op jit(solution)/shard_map/all_gather | solution.py:119
  88.3 5.8 %fusion.109 = bf16[2048,256]{0,1:T(8,128)(2,1)S(1)} fusion(bf16[2048,256]{1,0:T(8,128)(2,1)S(1)} %bitcast.317, bf16[1,2048,2048]{2,1,0:T(8,128)(2,1)} %all-gather.6.cloned.1.call-done), kind=kOutput, calls=%fused_computation.103 | convolution fusion | flops 2148007936 | bytes 10485760 | tf_op jit(solution)/shard_map/dot_general | solution.py:121
  95.1 1.6 reverse.3
  96.9 1.2 subtract_convert_fusion
  98.3 1.4 rev.14
  99.7 1.4 rev.13
  102.2 16.3 %while.31 = (s32[]{:T(128)}, f32[1,64,128]{2,1,0:T(8,128)S(1)}, f32[4,512,1,128]{3,1,0,2:T(8,128)S(1)}, f32[1,1,1]{2,1,0:T(1,128)}, bf16[4,512,1,64]{1,3,2,0:T(8...) while((s32[]{:T(128)}, f32[1,64,128]{2,1,0:T(8,128)S(1)}, ...), condition=%wide.region_3.4_spmd.clone.clone.clone, body=%wide.region_2.3_spmd.clone.clone.clone.sunk | while | flops 119506944 | bytes 2469500 | solution.py:81
  102.2 2.1 %fusion.158 = f32[128,512]{1,0:T(8,128)S(1)} fusion(f32[]{:T(128)} %get-tuple-element.492, bf16[4,512,1,128]{3,1,2,0:T(8,128)(2,1)S(1)} %get-tuple-element.490, s32[]{:T(128)} %get-tuple-element.475, bf16[4,512,1,64]{1,3,2,0:T(8,128)(2,1)S(1)} %get-tuple-element.491, bf16[4,512,1,64]{1,3,2,0:T(8,128)(2,1)} %get-tuple-element.489), kind=kOutput, calls=%fused_computation.55.clone.1 | convolution fusion | flops 102498304 | bytes 526336 | tf_op jit(solution)/shard_map/while/body/eval_jaxpr/hij,jhv->ihv/dot_general | solution.py:66
  106.3 2.1 %fusion.158 = f32[128,512]{1,0:T(8,128)S(1)} fusion(f32[]{:T(128)} %get-tuple-element.492, bf16[4,512,1,128]{3,1,2,0:T(8,128)(2,1)S(1)} %get-tuple-element.490, s32[]{:T(128)} %get-tuple-element.475, bf16[4,512,1,64]{1,3,2,0:T(8,128)(2,1)S(1)} %get-tuple-element.491, bf16[4,512,1,64]{1,3,2,0:T(8,128)(2,1)} %get-tuple-element.489), kind=kOutput, calls=%fused_computation.55.clone.1 | convolution fusion | flops 102498304 | bytes 526336 | tf_op jit(solution)/shard_map/while/body/eval_jaxpr/hij,jhv->ihv/dot_general | solution.py:66
  110.4 2.1 %fusion.158 = f32[128,512]{1,0:T(8,128)S(1)} fusion(f32[]{:T(128)} %get-tuple-element.492, bf16[4,512,1,128]{3,1,2,0:T(8,128)(2,1)S(1)} %get-tuple-element.490, s32[]{:T(128)} %get-tuple-element.475, bf16[4,512,1,64]{1,3,2,0:T(8,128)(2,1)S(1)} %get-tuple-element.491, bf16[4,512,1,64]{1,3,2,0:T(8,128)(2,1)} %get-tuple-element.489), kind=kOutput, calls=%fused_computation.55.clone.1 | convolution fusion | flops 102498304 | bytes 526336 | tf_op jit(solution)/shard_map/while/body/eval_jaxpr/hij,jhv->ihv/dot_general | solution.py:66
  114.5 2.1 %fusion.158 = f32[128,512]{1,0:T(8,128)S(1)} fusion(f32[]{:T(128)} %get-tuple-element.492, bf16[4,512,1,128]{3,1,2,0:T(8,128)(2,1)S(1)} %get-tuple-element.490, s32[]{:T(128)} %get-tuple-element.475, bf16[4,512,1,64]{1,3,2,0:T(8,128)(2,1)S(1)} %get-tuple-element.491, bf16[4,512,1,64]{1,3,2,0:T(8,128)(2,1)} %get-tuple-element.489), kind=kOutput, calls=%fused_computation.55.clone.1 | convolution fusion | flops 102498304 | bytes 526336 | tf_op jit(solution)/shard_map/while/body/eval_jaxpr/hij,jhv->ihv/dot_general | solution.py:66
  119.8 17.9 %while.30 = (s32[]{:T(128)}, f32[1,64,128]{2,1,0:T(8,128)S(1)}, f32[4,512,1,128]{3,1,0,2:T(8,128)S(1)}, f32[1,1,1]{2,1,0:T(1,128)}, bf16[4,512,1,64]{1,3,2,0:T(8...) while((s32[]{:T(128)}, f32[1,64,128]{2,1,0:T(8,128)S(1)}, ...), condition=%wide.region_1.2_spmd.clone.clone.clone, body=%wide.region_0.1_spmd.clone.clone.clone.sunk | while | flops 119506944 | bytes 2469500 | solution.py:81
  119.8 2.3 %fusion.148 = f32[128,512]{1,0:T(8,128)S(1)} fusion(f32[]{:T(128)} %get-tuple-element.522, bf16[4,512,1,128]{3,1,2,0:T(8,128)(2,1)} %get-tuple-element.520, s32[]{:T(128)} %get-tuple-element.505, bf16[4,512,1,64]{1,3,2,0:T(8,128)(2,1)S(1)} %get-tuple-element.521, bf16[4,512,1,64]{1,3,2,0:T(8,128)(2,1)} %get-tuple-element.519), kind=kOutput, calls=%fused_computation.8.clone.1 | convolution fusion | flops 102498304 | bytes 526336 | tf_op jit(solution)/shard_map/while/body/eval_jaxpr/hij,jhv->ihv/dot_general | solution.py:66
  124.3 2.3 %fusion.148 = f32[128,512]{1,0:T(8,128)S(1)} fusion(f32[]{:T(128)} %get-tuple-element.522, bf16[4,512,1,128]{3,1,2,0:T(8,128)(2,1)} %get-tuple-element.520, s32[]{:T(128)} %get-tuple-element.505, bf16[4,512,1,64]{1,3,2,0:T(8,128)(2,1)S(1)} %get-tuple-element.521, bf16[4,512,1,64]{1,3,2,0:T(8,128)(2,1)} %get-tuple-element.519), kind=kOutput, calls=%fused_computation.8.clone.1 | convolution fusion | flops 102498304 | bytes 526336 | tf_op jit(solution)/shard_map/while/body/eval_jaxpr/hij,jhv->ihv/dot_general | solution.py:66
  127.7 1.1 fusion.147
  128.8 2.3 %fusion.148 = f32[128,512]{1,0:T(8,128)S(1)} fusion(f32[]{:T(128)} %get-tuple-element.522, bf16[4,512,1,128]{3,1,2,0:T(8,128)(2,1)} %get-tuple-element.520, s32[]{:T(128)} %get-tuple-element.505, bf16[4,512,1,64]{1,3,2,0:T(8,128)(2,1)S(1)} %get-tuple-element.521, bf16[4,512,1,64]{1,3,2,0:T(8,128)(2,1)} %get-tuple-element.519), kind=kOutput, calls=%fused_computation.8.clone.1 | convolution fusion | flops 102498304 | bytes 526336 | tf_op jit(solution)/shard_map/while/body/eval_jaxpr/hij,jhv->ihv/dot_general | solution.py:66
  132.2 1.1 fusion.147
  133.3 2.3 %fusion.148 = f32[128,512]{1,0:T(8,128)S(1)} fusion(f32[]{:T(128)} %get-tuple-element.522, bf16[4,512,1,128]{3,1,2,0:T(8,128)(2,1)} %get-tuple-element.520, s32[]{:T(128)} %get-tuple-element.505, bf16[4,512,1,64]{1,3,2,0:T(8,128)(2,1)S(1)} %get-tuple-element.521, bf16[4,512,1,64]{1,3,2,0:T(8,128)(2,1)} %get-tuple-element.519), kind=kOutput, calls=%fused_computation.8.clone.1 | convolution fusion | flops 102498304 | bytes 526336 | tf_op jit(solution)/shard_map/while/body/eval_jaxpr/hij,jhv->ihv/dot_general | solution.py:66
  136.7 1.1 fusion.147
  139.6 16.4 %all_to_all.10 = bf16[16,128,1,128]{3,1,2,0:T(8,128)(2,1)S(1)} all-to-all(bf16[16,128,1,128]{3,1,2,0:T(8,128)(2,1)S(1)} %constant_dynamic-update-slice_fusion.2), channel_id=1, replica_groups=mesh['sp'=16,'dp'=16] {'sp'}, dimensions={0} | all-to-all | bytes 1048576 | tf_op jit(solution)/shard_map/all_to_all | solution.py:128
  156.4 5.5 %fusion.112 = bf16[1,128,2048]{2,1,0:T(8,128)(2,1)} fusion(bf16[128,2048]{0,1:T(8,128)(2,1)S(1)} %bitcast.308, bf16[2048,2048]{1,0:T(8,128)(2,1)} %all-gather.4.cloned.1.call-done), kind=kOutput, calls=%fused_computation.105 | convolution fusion | flops 1074003968 | bytes 9437184 | tf_op jit(solution)/shard_map/dot_general | solution.py:131
  (91 shorter events, 22.4 us)
Async XLA Ops:
  6.5 1.5 copy-start
  6.5 81.7 %all-gather.6.cloned.1.call-start = ((), (), s32[]{:S(2)}) async-start(), calls=%async_computation.3 | async-start | bytes 8912896 | tf_op jit(solution)/shard_map/all_gather | solution.py:119
  7.3 149.1 %all-gather.4.cloned.1.call-start = ((), (), s32[]{:S(2)}) async-start(), calls=%async_computation.2 | async-start | bytes 8912896 | tf_op jit(solution)/shard_map/all_gather | solution.py:133
  10.1 33.2 %all-to-all-start = ((bf16[16,128,256]{2,1,0:T(8,128)(2,1)}), bf16[16,128,256]{2,1,0:T(8,128)(2,1)S(1)}, u32[]{:S(2)}, u32[]{:S(2)}) async-start(bf16[16,128,256]{2,1,0:T(8,128)(2,1)} %broadcast_in_dim.18), calls=%async_computation | async-start | bytes 2097152 | tf_op jit(solution)/shard_map/all_to_all | solution.py:20
Sparse Core Ops, SparseCore 0:
  9.8 78.4 all-gather.5
  90.1 53.8 all-gather.3
